TPU v7x, 32 devices: a whole 2x2x4 slice. The times are simulated.
32 devices in a mesh: fs: 16 (over z, y, x), tp: 2 (over core).
Axes of the slice: x: 2, y: 2, z: 4, core: 2. Of those that a mesh axis runs over, the one named last changes fastest.
Arguments:
- tokens: bfloat16 [4096, 2048], P('fs'), may hold values from -6 to 6
- routes: int32 [4096, 6], P('fs'), may hold values from 0 to 15, all different within a row; in each aligned block of 256 rows (0 to 255, 256 to 511, ...) at most 160 rows name the same one
- route_weights: float32 [4096, 6], P('fs'), may hold values from 0.1 to 1
- norm_gain: float32 [2048], P('fs'), may hold values from 0.1 to 1.9
- expert_gate: float32 [16, 2048, 1024], P(None, 'fs', 'tp'), may hold values from -0.125 to 0.125
- expert_up: float32 [16, 2048, 1024], P(None, 'fs', 'tp'), may hold values from -0.125 to 0.125
- expert_down: float32 [16, 2048, 1024], P(None, 'fs', 'tp'), may hold values from -0.1875 to 0.1875
- shared_gate: float32 [2048, 1024], P('fs', 'tp'), may hold values from -0.125 to 0.125
- shared_up: float32 [2048, 1024], P('fs', 'tp'), may hold values from -0.125 to 0.125
- shared_down: float32 [2048, 1024], P('fs', 'tp'), may hold values from -0.1875 to 0.1875
Outputs:
- layer_output: bfloat16 [4096, 2048], P('fs', 'tp')
- sample_gate: bfloat16 [16, 2048, 1024], P('fs', None, 'tp')
- sample_up: bfloat16 [16, 2048, 1024], P('fs', None, 'tp')
- sample_down: bfloat16 [16, 2048, 1024], P('fs', None, 'tp')
- common_gate: bfloat16 [2048, 1024], P(None, 'tp')
- common_up: bfloat16 [2048, 1024], P(None, 'tp')
- common_down: bfloat16 [2048, 1024], P(None, 'tp')
Inputs may be any that keep to these rules, and one draw needn't show every extreme that they name: `routes`: each row names 6 different experts. In each aligned block of 256 rows (the rows of one index of fs) no expert is named by more than 160 rows, a bound that some expert reaches in some blocks.
All inputs are finite; a program needn't handle non-finite values.
Results may differ from a plain program's by a relative error of at most 0.015.
Values may be sent and summed in bfloat16 or wider, within the bound.
A program may use at most 128 MiB of HBM per device.

v0:
```python
import jax
import jax.numpy as jnp
from jax import lax
from jax.sharding import PartitionSpec as P

EPSILON = 1e-06


def normalize(tokens):
    values = tokens.astype(jnp.float32)
    scale = lax.rsqrt(jnp.mean(values * values, axis=-1, keepdims=True) + EPSILON)
    return (values * scale).astype(jnp.bfloat16)


def body(
    tokens,
    routes,
    route_weights,
    norm_gain,
    expert_gate,
    expert_up,
    expert_down,
    shared_gate,
    shared_up,
    shared_down,
):
    tp_count = lax.axis_size("tp")
    tp_index = lax.axis_index("tp")
    fs_count = lax.axis_size("fs")
    tok_rows, width = tokens.shape
    experts = expert_gate.shape[0]
    share = tok_rows // tp_count
    own_experts = experts // fs_count
    normed = normalize(tokens)
    own_normed = lax.dynamic_slice_in_dim(normed, tp_index * share, share, 0)
    own_routes = lax.dynamic_slice_in_dim(routes, tp_index * share, share, 0)
    own_weights = lax.dynamic_slice_in_dim(route_weights, tp_index * share, share, 0)
    member = own_routes[None, :, :] == jnp.arange(experts, dtype=jnp.int32)[:, None, None]
    dense = jnp.sum(jnp.where(member, own_weights[None, :, :], 0.0), axis=2)
    gathered = lax.all_gather(own_normed, "fs", axis=0, tiled=True)
    dense_all = lax.all_gather(dense, "fs", axis=0, tiled=False)
    gain_rows = norm_gain[None, :, None]
    rounded = (
        (expert_gate * gain_rows).astype(jnp.bfloat16),
        (expert_up * gain_rows).astype(jnp.bfloat16),
        expert_down.astype(jnp.bfloat16),
    )
    sample_gate, sample_up, sample_down = (
        lax.all_to_all(rounded[0], "fs", split_axis=0, concat_axis=1, tiled=True),
        lax.all_to_all(rounded[1], "fs", split_axis=0, concat_axis=1, tiled=True),
        lax.all_to_all(rounded[2], "fs", split_axis=0, concat_axis=1, tiled=True),
    )
    common_gate, common_up, common_down = (
        lax.all_gather(
            (shared_gate * norm_gain[:, None]).astype(jnp.bfloat16), "fs", axis=0, tiled=True
        ),
        lax.all_gather(
            (shared_up * norm_gain[:, None]).astype(jnp.bfloat16), "fs", axis=0, tiled=True
        ),
        lax.all_gather(shared_down.astype(jnp.bfloat16), "fs", axis=0, tiled=True),
    )
    shared_gate_act = jnp.dot(normed, common_gate, preferred_element_type=jnp.float32)
    shared_up_act = jnp.dot(normed, common_up, preferred_element_type=jnp.float32)
    shared_hidden = (jax.nn.silu(shared_gate_act) * shared_up_act).astype(jnp.bfloat16)
    shared_part = jnp.einsum(
        "th,dh->td", shared_hidden, common_down, preferred_element_type=jnp.float32
    ).astype(jnp.bfloat16)
    shared_parts = lax.all_to_all(
        shared_part.reshape(tok_rows, tp_count, width // tp_count).transpose(1, 0, 2),
        "tp",
        split_axis=0,
        concat_axis=0,
        tiled=True,
    )
    shared_sum = jnp.sum(shared_parts.astype(jnp.float32), axis=0)
    scale_all = lax.dynamic_slice_in_dim(
        dense_all, lax.axis_index("fs") * own_experts, own_experts, 1
    )
    total = None
    for expert in range(own_experts):
        scale = scale_all[:, expert, :].reshape(-1)[:, None]
        for shift in range(tp_count):
            gate_w, up_w, down_w = (sample_gate[expert], sample_up[expert], sample_down[expert])
            if shift:
                ring = [(i, (i + shift) % tp_count) for i in range(tp_count)]
                gate_w, up_w, down_w = (
                    lax.ppermute(gate_w, "tp", ring),
                    lax.ppermute(up_w, "tp", ring),
                    lax.ppermute(down_w, "tp", ring),
                )
            gate = jnp.dot(gathered, gate_w, preferred_element_type=jnp.float32)
            upward = jnp.dot(gathered, up_w, preferred_element_type=jnp.float32)
            hidden = (jax.nn.silu(gate) * upward * scale).astype(jnp.bfloat16)
            part = jnp.einsum("rf,df->rd", hidden, down_w, preferred_element_type=jnp.float32)
            total = part if total is None else total + part
    routed = lax.psum_scatter(total.astype(jnp.bfloat16), "fs", scatter_dimension=0, tiled=True)
    routed = lax.all_to_all(routed, "tp", split_axis=1, concat_axis=0, tiled=True)
    layer_output = (routed.astype(jnp.float32) + shared_sum).astype(jnp.bfloat16)
    return (layer_output, sample_gate, sample_up, sample_down, common_gate, common_up, common_down)


def solution(mesh):
    return jax.shard_map(
        body,
        mesh=mesh,
        in_specs=(
            P("fs", None),
            P("fs", None),
            P("fs", None),
            P("fs"),
            P(None, "fs", "tp"),
            P(None, "fs", "tp"),
            P(None, "fs", "tp"),
            P("fs", "tp"),
            P("fs", "tp"),
            P("fs", "tp"),
        ),
        out_specs=(
            P("fs", "tp"),
            P("fs", None, "tp"),
            P("fs", None, "tp"),
            P("fs", None, "tp"),
            P(None, "tp"),
            P(None, "tp"),
            P(None, "tp"),
        ),
        check_vma=False,
    )
```

profile of v0, /device:TPU:11, one launch (start us, length us, event | category | flops | bytes accessed | tf_op | source)
XLA Modules:
  0.0 607.8 jit_solution(15371878558450184911)
XLA Ops:
  7.2 1.5 fusion
  8.8 1.5 fusion.1
  11.1 6.8 %multiply_convert_fusion.2 = (bf16[16,128,512]{2,1,0:T(8,128)(2,1)}, bf16[16,128,512]{2,1,0:T(8,128)(2,1)}) fusion(f32[16,128,512]{2,1,0:T(8,128)} %param.15, f32[128]{0:T(128)S(1)} %copy-done.8, f32[16,128,512]{2,1,0:T(8,128)} %param.14), kind=kLoop, calls=%fused_computation.3 | loop fusion | flops 4194304 | bytes 12583424 | tf_op jit(solution)/shard_map/convert_element_type | solution.py:45
  17.9 6.8 %all-to-all-start = ((bf16[16,128,512]{2,1,0:T(8,128)(2,1)}), bf16[16,128,512]{2,1,0:T(8,128)(2,1)S(1)}, u32[]{:S(2)}, u32[]{:S(2)}) async-start(bf16[16,128,512]{2,1,0:T(8,128)(2,1)} %get-tuple-element.8), calls=%async_computation | async-start | bytes 4194304 | tf_op jit(solution)/shard_map/all_to_all | solution.py:49
  24.7 1.8 multiply_convert_fusion.6
  26.5 74.4 %all-to-all-done = bf16[16,128,512]{2,1,0:T(8,128)(2,1)S(1)} async-done(((bf16[16,128,512]{2,1,0:T(8,128)(2,1)}), bf16[16,128,512]{2,1,0:T(8,128)(2,1)S(1)}, u32[]{:S(2)}, u32[]{:S(2)}) %all-to-all-start) | async-done | bytes 2097184 | tf_op jit(solution)/shard_map/all_to_all | solution.py:49
  101.0 6.9 %all-to-all-start.1 = ((bf16[16,128,512]{2,1,0:T(8,128)(2,1)}), bf16[16,128,512]{2,1,0:T(8,128)(2,1)}, u32[]{:S(2)}, u32[]{:S(2)}) async-start(bf16[16,128,512]{2,1,0:T(8,128)(2,1)} %get-tuple-element.7), calls=%async_computation.1 | async-start | bytes 4194304 | tf_op jit(solution)/shard_map/all_to_all | solution.py:50
  108.6 3.9 convert_element_type.59
  112.5 81.0 %all-to-all-done.1 = bf16[16,128,512]{2,1,0:T(8,128)(2,1)} async-done(((bf16[16,128,512]{2,1,0:T(8,128)(2,1)}), bf16[16,128,512]{2,1,0:T(8,128)(2,1)}, u32[]{:S(2)}, u32[]{:S(2)}) %all-to-all-start.1) | async-done | bytes 2097184 | tf_op jit(solution)/shard_map/all_to_all | solution.py:50
  193.5 9.3 %all-to-all-start.2 = ((bf16[16,128,512]{2,1,0:T(8,128)(2,1)}), bf16[16,128,512]{2,1,0:T(8,128)(2,1)}, u32[]{:S(2)}, u32[]{:S(2)}) async-start(bf16[16,128,512]{2,1,0:T(8,128)(2,1)} %convert_element_type.59), calls=%async_computation.2 | async-start | bytes 4194304 | tf_op jit(solution)/shard_map/all_to_all | solution.py:51
  202.8 4.0 collective-permute-start
  207.7 68.8 %all-gather = f32[256,128]{1,0:T(8,128)S(1)} all-gather(f32[16,128]{1,0:T(8,128)S(1)} %select_reduce_fusion), channel_id=2, replica_groups=mesh['fs'=16,'tp'=2] {'fs'}, dimensions={0}, use_global_device_ids=true | all-gather | bytes 139264 | tf_op jit(solution)/shard_map/all_gather | solution.py:41
  276.5 8.9 %collective-permute-start.1 = (bf16[2048,512]{1,0:T(8,128)(2,1)}, bf16[2048,512]{1,0:T(8,128)(2,1)}, u32[]{:S(2)}, u32[]{:S(2)}) collective-permute-start(bf16[2048,512]{1,0:T(8,128)(2,1)} %bitcast.1), channel_id=1, source_target_pairs={{0,1},{1,0},{2,3},{3,2},{4,5},{5,4},{6,7},{7,6},{8,9},{9,8},{10,11... | collective-permute-start | bytes 6291464 | tf_op jit(solution)/shard_map/ppermute | solution.py:88
  285.5 9.8 %fusion.16 = f32[2048,512]{1,0:T(8,128)} fusion(bf16[2048,2048]{1,0:T(8,128)(2,1)} %all-gather.6.cloned.1.call-done, bf16[2048,512]{1,0:T(8,128)(2,1)S(1)} %bitcast.41), kind=kOutput, calls=%fused_computation.38 | convolution fusion | flops 4294967296 | bytes 14680064 | tf_op jit(solution)/shard_map/dot_general | solution.py:91
  295.3 7.6 %fusion.17 = f32[2048,512]{1,0:T(8,128)} fusion(bf16[2048,2048]{1,0:T(8,128)(2,1)S(1)} %copy-done.9, bf16[2048,512]{1,0:T(8,128)(2,1)} %collective-permute-done), kind=kOutput, calls=%fused_computation.39 | convolution fusion | flops 4294967296 | bytes 14680064 | tf_op jit(solution)/shard_map/dot_general | solution.py:91
  302.9 7.6 %fusion.18 = f32[2048,512]{1,0:T(8,128)} fusion(bf16[2048,2048]{1,0:T(8,128)(2,1)S(1)} %copy-done.9, bf16[2048,512]{1,0:T(8,128)(2,1)} %collective-permute-done.1), kind=kOutput, calls=%fused_computation.40 | convolution fusion | flops 4294967296 | bytes 14680064 | tf_op jit(solution)/shard_map/dot_general | solution.py:92
  310.5 16.6 %fusion.6 = f32[2048,2048]{1,0:T(8,128)} fusion(bf16[2048,512]{1,0:T(8,128)(2,1)} %bitcast.4, f32[2048,512]{1,0:T(8,128)} %fusion.16, bf16[2048,2048]{1,0:T(8,128)(2,1)} %all-gather.6.cloned.1.call-done, bf16[2048,512]{1,0:T(8,128)(2,1)} %bitcast.1, f32[2048]{0:T(1024)S(1)} %bitcast.48), kind=kOutput, calls=%fused_computation.18 | convolution fusion | flops 8597274624 | bytes 33562624 | tf_op jit(solution)/shard_map/rf,df->rd/dot_general | solution.py:94
  327.0 13.6 %add_convert_fusion = bf16[2048,2048]{1,0:T(8,128)(2,1)} fusion(f32[2048,2048]{1,0:T(8,128)} %fusion.6, bf16[2048,512]{1,0:T(8,128)(2,1)} %collective-permute-done.2, f32[2048,512]{1,0:T(8,128)} %fusion.18, f32[2048,512]{1,0:T(8,128)} %fusion.17, f32[2048]{0:T(1024)S(1)} %bitcast.49), kind=kOutput, calls=%fused_computation | convolution fusion | flops 4310695936 | bytes 35659776 | tf_op jit(solution)/shard_map/rf,df->rd/dot_general | solution.py:94
  340.7 3.1 fusion.19
  343.8 55.0 %all-gather.12.cloned.1.call-done = bf16[2048,512]{1,0:T(8,128)(2,1)} async-done(((bf16[128,512]{1,0:T(8,128)(2,1)}), bf16[2048,512]{1,0:T(8,128)(2,1)}) %all-gather.12.cloned.1.call-update) | async-done | bytes 2097168 | tf_op jit(solution)/shard_map/all_gather | solution.py:60
  398.8 4.7 convolution_convert_fusion
  403.5 2.3 copy.30
  405.7 5.2 all-to-all-start.4
  410.9 1.7 all-to-all-done.4
  413.9 167.8 %reduce-scatter.2.cloned.1.call-done = bf16[128,2048]{1,0:T(8,128)(2,1)} async-done(((bf16[2048,2048]{1,0:T(8,128)(2,1)}), bf16[128,2048]{1,0:T(8,128)(2,1)}) %reduce-scatter.2.cloned.1.call-update) | async-done | bytes 524304 | tf_op jit(solution)/shard_map/reduce_scatter | solution.py:96
  582.8 4.7 all_to_all.54
  587.4 2.2 fusion.5
  590.9 3.2 copy.39
  594.1 3.2 copy.40
  597.3 1.3 copy.41
  598.7 1.3 copy.42
  600.0 1.3 copy.43
  (48 shorter events, 6.2 us)
Async XLA Ops:
  7.2 200.4 %copy-start = (f32[256,6]{0,1:T(8,128)S(1)}, f32[256,6]{0,1:T(8,128)}, u32[]{:S(2)}) copy-start(f32[256,6]{0,1:T(8,128)} %param.12) | copy-start | bytes 18436
  7.2 3.9 copy-start.8
  7.2 278.3 %all-gather.6.cloned.1.call-start = ((), (), s32[]{:S(2)}) async-start(), calls=%async_computation.6 | async-start | bytes 8912896 | tf_op jit(solution)/shard_map/all_gather | solution.py:40
  17.9 6.8 %copy-start.6 = (f32[128,512]{1,0:T(8,128)S(1)}, f32[128,512]{1,0:T(8,128)}, u32[]{:S(2)}) copy-start(f32[128,512]{1,0:T(8,128)} %param.17) | copy-start | bytes 786436
  17.9 83.0 %all-to-all-start = ((bf16[16,128,512]{2,1,0:T(8,128)(2,1)}), bf16[16,128,512]{2,1,0:T(8,128)(2,1)S(1)}, u32[]{:S(2)}, u32[]{:S(2)}) async-start(bf16[16,128,512]{2,1,0:T(8,128)(2,1)} %get-tuple-element.8), calls=%async_computation | async-start | bytes 4194304 | tf_op jit(solution)/shard_map/all_to_all | solution.py:49
  24.7 316.0 %all-gather.8.cloned.1.call-start = ((), (), s32[]{:S(2)}) async-start(), calls=%async_computation.8 | async-start | bytes 2228224 | tf_op jit(solution)/shard_map/all_gather | solution.py:54
  101.0 92.5 %all-to-all-start.1 = ((bf16[16,128,512]{2,1,0:T(8,128)(2,1)}), bf16[16,128,512]{2,1,0:T(8,128)(2,1)}, u32[]{:S(2)}, u32[]{:S(2)}) async-start(bf16[16,128,512]{2,1,0:T(8,128)(2,1)} %get-tuple-element.7), calls=%async_computation.1 | async-start | bytes 4194304 | tf_op jit(solution)/shard_map/all_to_all | solution.py:50
  107.8 235.9 %all-gather.10.cloned.1.call-start = ((), (), s32[]{:S(2)}) async-start(), calls=%async_computation.9 | async-start | bytes 2228224 | tf_op jit(solution)/shard_map/all_gather | solution.py:57
  108.6 98.3 %copy-start.5 = (f32[128,512]{1,0:T(8,128)S(1)}, f32[128,512]{1,0:T(8,128)}, u32[]{:S(2)}) copy-start(f32[128,512]{1,0:T(8,128)} %param.19) | copy-start | bytes 786436
  108.6 99.1 %copy-start.7 = (s32[256,6]{0,1:T(8,128)S(1)}, s32[256,6]{0,1:T(8,128)}, u32[]{:S(2)}) copy-start(s32[256,6]{0,1:T(8,128)} %param.11) | copy-start | bytes 18436
  193.5 91.9 %all-to-all-start.2 = ((bf16[16,128,512]{2,1,0:T(8,128)(2,1)}), bf16[16,128,512]{2,1,0:T(8,128)(2,1)}, u32[]{:S(2)}, u32[]{:S(2)}) async-start(bf16[16,128,512]{2,1,0:T(8,128)(2,1)} %convert_element_type.59), calls=%async_computation.2 | async-start | bytes 4194304 | tf_op jit(solution)/shard_map/all_to_all | solution.py:51
  202.8 196.0 %all-gather.12.cloned.1.call-start = ((), (), s32[]{:S(2)}) async-start(), calls=%async_computation.10 | async-start | bytes 2228224 | tf_op jit(solution)/shard_map/all_gather | solution.py:60
  202.8 92.5 %collective-permute-start = (bf16[2048,512]{1,0:T(8,128)(2,1)S(1)}, bf16[2048,512]{1,0:T(8,128)(2,1)}, u32[]{:S(2)}, u32[]{:S(2)}) collective-permute-start(bf16[2048,512]{1,0:T(8,128)(2,1)S(1)} %bitcast.40), channel_id=1, source_target_pairs={{0,1},{1,0},{2,3},{3,2},{4,5},{5,4},{6,7},{7,6},{8,9},{9,8},{10,11... | collective-permute-start | bytes 6291464 | tf_op jit(solution)/shard_map/ppermute | solution.py:87
  207.5 374.1 %reduce-scatter.2.cloned.1.call-start = ((), (), s32[]{:S(2)}) async-start(), calls=%async_computation.7 | async-start | bytes 8912896 | tf_op jit(solution)/shard_map/reduce_scatter | solution.py:96
  276.5 26.4 %collective-permute-start.1 = (bf16[2048,512]{1,0:T(8,128)(2,1)}, bf16[2048,512]{1,0:T(8,128)(2,1)}, u32[]{:S(2)}, u32[]{:S(2)}) collective-permute-start(bf16[2048,512]{1,0:T(8,128)(2,1)} %bitcast.1), channel_id=1, source_target_pairs={{0,1},{1,0},{2,3},{3,2},{4,5},{5,4},{6,7},{7,6},{8,9},{9,8},{10,11... | collective-permute-start | bytes 6291464 | tf_op jit(solution)/shard_map/ppermute | solution.py:88
  285.4 41.6 %collective-permute-start.2 = (bf16[2048,512]{1,0:T(8,128)(2,1)}, bf16[2048,512]{1,0:T(8,128)(2,1)}, u32[]{:S(2)}, u32[]{:S(2)}) collective-permute-start(bf16[2048,512]{1,0:T(8,128)(2,1)} %bitcast.4), channel_id=1, source_target_pairs={{0,1},{1,0},{2,3},{3,2},{4,5},{5,4},{6,7},{7,6},{8,9},{9,8},{10,11... | collective-permute-start | bytes 6291464 | tf_op jit(solution)/shard_map/ppermute | solution.py:89
  285.5 9.8 %copy-start.9 = (bf16[2048,2048]{1,0:T(8,128)(2,1)S(1)}, bf16[2048,2048]{1,0:T(8,128)(2,1)}, u32[]{:S(2)}) copy-start(bf16[2048,2048]{1,0:T(8,128)(2,1)} %all-gather.6.cloned.1.call-done) | copy-start | bytes 25165828
  405.7 6.9 %all-to-all-start.4 = ((bf16[2,256,1024]{2,1,0:T(8,128)(2,1)}), bf16[2,256,1024]{2,1,0:T(8,128)(2,1)S(1)}, u32[]{:S(2)}, u32[]{:S(2)}) async-start(bf16[2,256,1024]{2,1,0:T(8,128)(2,1)} %bitcast.43), calls=%async_computation.5 | async-start | bytes 2097152 | tf_op jit(solution)/shard_map/all_to_all | solution.py:68
  590.9 6.4 %copy-start.2 = (bf16[2048,512]{1,0:T(8,128)(2,1)S(1)}, bf16[2048,512]{1,0:T(8,128)(2,1)}, u32[]{:S(2)}) copy-start(bf16[2048,512]{1,0:T(8,128)(2,1)} %all-gather.8.cloned.1.call-done) | copy-start | bytes 6291460
  594.1 4.5 copy-start.3
  597.3 2.6 copy-start.4
  597.3 4.0 copy-start.1
Sparse Core Ops, SparseCore 0:
  11.3 187.2 all-gather.5
  202.0 71.4 all-gather.7
  276.8 59.5 all-gather.9
  339.6 59.1 all-gather.11
  400.9 180.7 reduce-scatter.1
where the time goes:
time: 609 us; the launch traced here: 608 us
  waiting for transfers between devices  381 us (63%)
  blocking collectives  73.5 us (12%)
  matrix products  62.9 us (10%)
  starting transfers between devices  41.3 us (7%)
  other arithmetic  19.5 us (3%)
  local copies, waits for them, and re-layouts  15.9 us (3%)
  between operations  13.9 us (2%)
    reduce_scatter x1, waiting for transfers between devices, body(): lax.psum_scatter(total.astype(jnp.bfloat16), 'fs', scatter_dimension=0, t...  168 us
    all_to_all x1, waiting for transfers between devices, body(): lax.all_to_all(rounded[1], 'fs', split_axis=0, concat_axis=1, tiled=True)  81 us
    all_to_all x1, waiting for transfers between devices, body(): lax.all_to_all(rounded[0], 'fs', split_axis=0, concat_axis=1, tiled=True)  74.4 us
    all_gather x1, blocking collectives, body(): dense_all = lax.all_gather(dense, 'fs', axis=0, tiled=False)  68.8 us
    all_gather x1, waiting for transfers between devices, body(): lax.all_gather(shared_down.astype(jnp.bfloat16), 'fs', axis=0, tiled=True)  55 us
    dot_general x2, matrix products, body(): jnp.einsum('rf,df->rd', hidden, down_w, preferred_element_type=jnp.float32)  30.1 us
    dot_general x2, matrix products, body(): gate = jnp.dot(gathered, gate_w, preferred_element_type=jnp.float32)  17.4 us
  transfers between devices with their start and end apart: 12, of which 5 were waited for; matrix products, arithmetic and copies ran while one was open for 13% of the time, Pallas kernels for 0%

commit v1 on v0

--- a/solution.py
+++ b/solution.py
@@ -4,6 +4,38 @@
 from jax.sharding import PartitionSpec as P
 
 EPSILON = 1e-06
+
+
+def part_the_patch(inp, dimension_no):
+    inp = jnp.moveaxis(inp, 0, dimension_no)
+    newest = inp.shape
+    return inp.reshape(
+        *newest[:dimension_no],
+        newest[dimension_no] * newest[dimension_no + 1],
+        *newest[dimension_no + 2 :]
+    )
+
+
+def points_try_all(unit, axis_name, d_out):
+    amount_of = lax.axis_size(axis_name)
+    gallery = [(d, (d + 1) % amount_of) for d in range(amount_of)]
+    plain, carry_out = ([], [])
+    rr = 0
+    frames = [(num, dev_i) for dev_i, num in gallery]
+    while rr < amount_of - 1:
+        if rr % 2 == 0:
+            plain.append(
+                lax.ppermute(plain[-1] if plain else unit, axis_name=axis_name, perm=gallery)
+            )
+        else:
+            carry_out.append(
+                lax.ppermute(carry_out[-1] if carry_out else unit, axis_name=axis_name, perm=frames)
+            )
+        rr += 1
+    shaped = jnp.stack([*plain[::-1], unit, *carry_out])
+    tile_out = lax.axis_index(axis_name) - len(plain)
+    shaped = shaped[(jnp.arange(amount_of) - tile_out) % amount_of]
+    return part_the_patch(shaped, d_out)
 
 
 def normalize(tokens):
@@ -57,7 +89,7 @@
         lax.all_gather(
             (shared_up * norm_gain[:, None]).astype(jnp.bfloat16), "fs", axis=0, tiled=True
         ),
-        lax.all_gather(shared_down.astype(jnp.bfloat16), "fs", axis=0, tiled=True),
+        points_try_all(shared_down.astype(jnp.bfloat16), "fs", 0),
     )
     shared_gate_act = jnp.dot(normed, common_gate, preferred_element_type=jnp.float32)
     shared_up_act = jnp.dot(normed, common_up, preferred_element_type=jnp.float32)

time: 609 us -> 586 us (0.962)
  waiting for transfers between devices: 381 us -> 249 us
  blocking collectives: 73.5 us -> 163 us
  local copies, waits for them, and re-layouts: 15.9 us -> 39.2 us
    reduce_scatter x1, waiting for transfers between devices: 168 us -> 77.6 us  [body(): lax.psum_scatter(total.astype(jnp.bfloat16), 'fs', scatter_dimension=0, t...]
    ppermute x0 -> x15, waiting for transfers between devices: none -> 88.3 us  [the longest x8 56.5 us: points_try_all(): lax.ppermute(plain[-1] if plain else unit, axis_name=axis_name, perm=gall...]
    all_to_all x0 -> x1, blocking collectives: none -> 85.9 us  [body(): lax.all_to_all(rounded[0], 'fs', split_axis=0, concat_axis=1, tiled=True)]
    all_to_all x1 -> x0, waiting for transfers between devices: 74.4 us -> none  [body(): lax.all_to_all(rounded[0], 'fs', split_axis=0, concat_axis=1, tiled=True)]
    all_gather x1 -> x0, waiting for transfers between devices: 55 us -> none  [body(): lax.all_gather(shared_down.astype(jnp.bfloat16), 'fs', axis=0, tiled=True)]
    unnamed x26 -> x59, local copies, waits for them, and re-layouts: 11.7 us -> 30.7 us
    ppermute x0 -> x15, starting transfers between devices: none -> 14.3 us  [the longest x8 12.3 us: points_try_all(): lax.ppermute(plain[-1] if plain else unit, axis_name=axis_name, perm=gall...]
    all_to_all x1 -> x0, starting transfers between devices: 6.77 us -> none  [body(): lax.all_to_all(rounded[0], 'fs', split_axis=0, concat_axis=1, tiled=True)]
  transfers between devices with their start and end apart: 12 -> 25, of which waited for: 5 -> 16; matrix products, arithmetic and copies ran while one was open for 13% -> 17% of each run, Pallas kernels for 0% -> 0%
where the time goes in v1:
time: 586 us; the launch traced here: 585 us
  waiting for transfers between devices  249 us (42%)
  blocking collectives  163 us (28%)
  matrix products  63 us (11%)
  starting transfers between devices  39.6 us (7%)
  local copies, waits for them, and re-layouts  39.2 us (7%)
  other arithmetic  17.6 us (3%)
  between operations  14 us (2%)
    all_to_all x1, blocking collectives, body(): lax.all_to_all(rounded[0], 'fs', split_axis=0, concat_axis=1, tiled=True)  85.9 us
    all_to_all x1, waiting for transfers between devices, body(): lax.all_to_all(rounded[1], 'fs', split_axis=0, concat_axis=1, tiled=True)  80.8 us
    reduce_scatter x1, waiting for transfers between devices, body(): lax.psum_scatter(total.astype(jnp.bfloat16), 'fs', scatter_dimension=0, t...  77.6 us
    all_gather x1, blocking collectives, body(): dense_all = lax.all_gather(dense, 'fs', axis=0, tiled=False)  72.3 us
    ppermute x8, waiting for transfers between devices, points_try_all(): lax.ppermute(plain[-1] if plain else unit, axis_name=axis_name, perm=gall...  56.5 us
    ppermute x7, waiting for transfers between devices, points_try_all(): lax.ppermute(carry_out[-1] if carry_out else unit, axis_name=axis_name, p...  31.8 us
    unnamed x59, local copies, waits for them, and re-layouts  30.7 us
    dot_general x2, matrix products, body(): jnp.einsum('rf,df->rd', hidden, down_w, preferred_element_type=jnp.float32)  30.2 us
  transfers between devices with their start and end apart: 25, of which 16 were waited for; matrix products, arithmetic and copies ran while one was open for 17% of the time, Pallas kernels for 0%

profile of v1, /device:TPU:11, one launch (start us, length us, event | category | flops | bytes accessed | tf_op | source)
XLA Modules:
  0.0 584.9 jit_solution(2468014008433568807)
XLA Ops:
  11.1 6.1 %multiply_convert_fusion.2 = (bf16[16,128,512]{2,1,0:T(8,128)(2,1)}, bf16[16,128,512]{2,1,0:T(8,128)(2,1)S(1)}) fusion(f32[16,128,512]{2,1,0:T(8,128)} %param.15, f32[128]{0:T(128)S(1)} %copy-done.18, f32[16,128,512]{2,1,0:T(8,128)} %param.14), kind=kLoop, calls=%fused_computation.4 | loop fusion | flops 4194304 | bytes 12583424 | tf_op jit(solution)/shard_map/convert_element_type | solution.py:77
  17.2 85.9 %all_to_all.54 = bf16[16,128,512]{2,1,0:T(8,128)(2,1)S(1)} all-to-all(bf16[16,128,512]{2,1,0:T(8,128)(2,1)S(1)} %get-tuple-element.8), channel_id=1, replica_groups=mesh['fs'=16,'tp'=2] {'fs'}, dimensions={0} | all-to-all | bytes 4194304 | tf_op jit(solution)/shard_map/all_to_all | solution.py:81
  103.2 5.2 all-to-all-start.1
  110.2 3.8 convert_element_type.59
  114.0 80.8 %all-to-all-done.1 = bf16[16,128,512]{2,1,0:T(8,128)(2,1)} async-done(((bf16[16,128,512]{2,1,0:T(8,128)(2,1)}), bf16[16,128,512]{2,1,0:T(8,128)(2,1)}, u32[]{:S(2)}, u32[]{:S(2)}) %all-to-all-start.1) | async-done | bytes 2097184 | tf_op jit(solution)/shard_map/all_to_all | solution.py:82
  194.8 7.4 %all-to-all-start.2 = ((bf16[16,128,512]{2,1,0:T(8,128)(2,1)}), bf16[16,128,512]{2,1,0:T(8,128)(2,1)}, u32[]{:S(2)}, u32[]{:S(2)}) async-start(bf16[16,128,512]{2,1,0:T(8,128)(2,1)} %convert_element_type.59), calls=%async_computation.2 | async-start | bytes 4194304 | tf_op jit(solution)/shard_map/all_to_all | solution.py:83
  203.5 72.3 %all-gather = f32[256,128]{1,0:T(8,128)S(1)} all-gather(f32[16,128]{1,0:T(8,128)S(1)} %select_reduce_fusion), channel_id=2, replica_groups=mesh['fs'=16,'tp'=2] {'fs'}, dimensions={0}, use_global_device_ids=true | all-gather | bytes 139264 | tf_op jit(solution)/shard_map/all_gather | solution.py:73
  275.8 6.8 %collective-permute-start.1 = (bf16[2048,512]{1,0:T(8,128)(2,1)}, bf16[2048,512]{1,0:T(8,128)(2,1)}, u32[]{:S(2)}, u32[]{:S(2)}) collective-permute-start(bf16[2048,512]{1,0:T(8,128)(2,1)} %bitcast.1), channel_id=1, source_target_pairs={{0,1},{1,0},{2,3},{3,2},{4,5},{5,4},{6,7},{7,6},{8,9},{9,8},{10,11... | collective-permute-start | bytes 6291464 | tf_op jit(solution)/shard_map/ppermute | solution.py:120
  282.8 9.7 %fusion.18 = f32[2048,512]{1,0:T(8,128)} fusion(bf16[2048,2048]{1,0:T(8,128)(2,1)} %all-gather.5.cloned.1.call-done, bf16[2048,512]{1,0:T(8,128)(2,1)S(1)} %bitcast.76), kind=kOutput, calls=%fused_computation.62 | convolution fusion | flops 4294967296 | bytes 14680064 | tf_op jit(solution)/shard_map/dot_general | solution.py:123
  292.4 7.7 %fusion.19 = f32[2048,512]{1,0:T(8,128)} fusion(bf16[2048,2048]{1,0:T(8,128)(2,1)S(1)} %copy-done.19, bf16[2048,512]{1,0:T(8,128)(2,1)} %collective-permute-done), kind=kOutput, calls=%fused_computation.63 | convolution fusion | flops 4294967296 | bytes 14680064 | tf_op jit(solution)/shard_map/dot_general | solution.py:123
  300.1 7.6 %fusion.20 = f32[2048,512]{1,0:T(8,128)} fusion(bf16[2048,2048]{1,0:T(8,128)(2,1)S(1)} %copy-done.19, bf16[2048,512]{1,0:T(8,128)(2,1)} %collective-permute-done.1), kind=kOutput, calls=%fused_computation.64 | convolution fusion | flops 4294967296 | bytes 14680064 | tf_op jit(solution)/shard_map/dot_general | solution.py:124
  307.7 16.7 %fusion.6 = f32[2048,2048]{1,0:T(8,128)} fusion(bf16[2048,512]{1,0:T(8,128)(2,1)} %bitcast.4, f32[2048,512]{1,0:T(8,128)} %fusion.18, bf16[2048,2048]{1,0:T(8,128)(2,1)} %all-gather.5.cloned.1.call-done, bf16[2048,512]{1,0:T(8,128)(2,1)} %bitcast.1, f32[2048]{0:T(1024)S(1)} %bitcast.85), kind=kOutput, calls=%fused_computation.19 | convolution fusion | flops 8597274624 | bytes 33562624 | tf_op jit(solution)/shard_map/rf,df->rd/dot_general | solution.py:126
  324.4 13.5 %add_convert_fusion = bf16[2048,2048]{1,0:T(8,128)(2,1)} fusion(f32[2048,2048]{1,0:T(8,128)} %fusion.6, bf16[2048,512]{1,0:T(8,128)(2,1)} %collective-permute-done.2, f32[2048,512]{1,0:T(8,128)} %fusion.20, f32[2048,512]{1,0:T(8,128)} %fusion.19, f32[2048]{0:T(1024)S(1)} %bitcast.86), kind=kOutput, calls=%fused_computation.1 | convolution fusion | flops 4310695936 | bytes 35659776 | tf_op jit(solution)/shard_map/rf,df->rd/dot_general | solution.py:126
  346.8 14.7 %collective-permute-done.4 = bf16[128,512]{1,0:T(8,128)(2,1)S(1)} collective-permute-done((bf16[128,512]{1,0:T(8,128)(2,1)S(1)}, bf16[128,512]{1,0:T(8,128)(2,1)S(1)}, u32[]{:S(2)}, u32[]{:S(2)}) %collective-permute-start.4) | collective-permute-done | bytes 131104 | tf_op jit(solution)/shard_map/ppermute | solution.py:28
  363.6 8.7 %collective-permute-done.5 = bf16[128,512]{1,0:T(8,128)(2,1)S(1)} collective-permute-done((bf16[128,512]{1,0:T(8,128)(2,1)S(1)}, bf16[128,512]{1,0:T(8,128)(2,1)S(1)}, u32[]{:S(2)}, u32[]{:S(2)}) %collective-permute-start.5) | collective-permute-done | bytes 131104 | tf_op jit(solution)/shard_map/ppermute | solution.py:28
  374.4 6.2 %collective-permute-done.12 = bf16[128,512]{1,0:T(8,128)(2,1)S(1)} collective-permute-done((bf16[128,512]{1,0:T(8,128)(2,1)S(1)}, bf16[128,512]{1,0:T(8,128)(2,1)S(1)}, u32[]{:S(2)}, u32[]{:S(2)}) %collective-permute-start.12) | collective-permute-done | bytes 131104 | tf_op jit(solution)/shard_map/ppermute | solution.py:32
  381.2 4.4 collective-permute-done.6
  387.9 6.3 %collective-permute-done.13 = bf16[128,512]{1,0:T(8,128)(2,1)S(1)} collective-permute-done((bf16[128,512]{1,0:T(8,128)(2,1)S(1)}, bf16[128,512]{1,0:T(8,128)(2,1)S(1)}, u32[]{:S(2)}, u32[]{:S(2)}) %collective-permute-start.13) | collective-permute-done | bytes 131104 | tf_op jit(solution)/shard_map/ppermute | solution.py:32
  394.9 6.2 %collective-permute-done.7 = bf16[128,512]{1,0:T(8,128)(2,1)S(1)} collective-permute-done((bf16[128,512]{1,0:T(8,128)(2,1)S(1)}, bf16[128,512]{1,0:T(8,128)(2,1)S(1)}, u32[]{:S(2)}, u32[]{:S(2)}) %collective-permute-start.7) | collective-permute-done | bytes 131104 | tf_op jit(solution)/shard_map/ppermute | solution.py:28
  402.3 6.3 %collective-permute-done.14 = bf16[128,512]{1,0:T(8,128)(2,1)} collective-permute-done((bf16[128,512]{1,0:T(8,128)(2,1)S(1)}, bf16[128,512]{1,0:T(8,128)(2,1)}, u32[]{:S(2)}, u32[]{:S(2)}) %collective-permute-start.14) | collective-permute-done | bytes 131104 | tf_op jit(solution)/shard_map/ppermute | solution.py:32
  408.6 8.0 %collective-permute-done.8 = bf16[128,512]{1,0:T(8,128)(2,1)} collective-permute-done((bf16[128,512]{1,0:T(8,128)(2,1)S(1)}, bf16[128,512]{1,0:T(8,128)(2,1)}, u32[]{:S(2)}, u32[]{:S(2)}) %collective-permute-start.8) | collective-permute-done | bytes 131104 | tf_op jit(solution)/shard_map/ppermute | solution.py:28
  416.6 6.2 %collective-permute-done.15 = bf16[128,512]{1,0:T(8,128)(2,1)} collective-permute-done((bf16[128,512]{1,0:T(8,128)(2,1)}, bf16[128,512]{1,0:T(8,128)(2,1)}, u32[]{:S(2)}, u32[]{:S(2)}) %collective-permute-start.15) | collective-permute-done | bytes 131104 | tf_op jit(solution)/shard_map/ppermute | solution.py:32
  422.8 6.0 %collective-permute-done.9 = bf16[128,512]{1,0:T(8,128)(2,1)} collective-permute-done((bf16[128,512]{1,0:T(8,128)(2,1)}, bf16[128,512]{1,0:T(8,128)(2,1)}, u32[]{:S(2)}, u32[]{:S(2)}) %collective-permute-start.9) | collective-permute-done | bytes 131104 | tf_op jit(solution)/shard_map/ppermute | solution.py:28
  431.2 6.8 %collective-permute-done.16 = bf16[128,512]{1,0:T(8,128)(2,1)S(1)} collective-permute-done((bf16[128,512]{1,0:T(8,128)(2,1)}, bf16[128,512]{1,0:T(8,128)(2,1)S(1)}, u32[]{:S(2)}, u32[]{:S(2)}) %collective-permute-start.16) | collective-permute-done | bytes 131104 | tf_op jit(solution)/shard_map/ppermute | solution.py:32
  438.0 5.6 collective-permute-done.10
  461.5 3.6 gather_fusion
  465.1 3.1 fusion.21
  468.2 4.7 convolution_convert_fusion
  475.2 4.6 all-to-all-start.4
  482.7 77.6 %reduce-scatter.2.cloned.1.call-done = bf16[128,2048]{1,0:T(8,128)(2,1)} async-done(((bf16[2048,2048]{1,0:T(8,128)(2,1)}), bf16[128,2048]{1,0:T(8,128)(2,1)}) %reduce-scatter.2.cloned.1.call-update) | async-done | bytes 524304 | tf_op jit(solution)/shard_map/reduce_scatter | solution.py:128
  561.4 4.8 all_to_all.55
  571.5 3.2 copy.54
  (112 shorter events, 60.5 us)
Async XLA Ops:
  7.2 196.2 %copy-start = (f32[256,6]{0,1:T(8,128)S(1)}, f32[256,6]{0,1:T(8,128)}, u32[]{:S(2)}) copy-start(f32[256,6]{0,1:T(8,128)} %param.12) | copy-start | bytes 18436
  7.2 275.6 %all-gather.5.cloned.1.call-start = ((), (), s32[]{:S(2)}) async-start(), calls=%async_computation.6 | async-start | bytes 8912896 | tf_op jit(solution)/shard_map/all_gather | solution.py:72
  103.2 91.6 %all-to-all-start.1 = ((bf16[16,128,512]{2,1,0:T(8,128)(2,1)}), bf16[16,128,512]{2,1,0:T(8,128)(2,1)}, u32[]{:S(2)}, u32[]{:S(2)}) async-start(bf16[16,128,512]{2,1,0:T(8,128)(2,1)} %get-tuple-element.7), calls=%async_computation.1 | async-start | bytes 4194304 | tf_op jit(solution)/shard_map/all_to_all | solution.py:82
  108.3 356.8 %all-gather.7.cloned.1.call-start = ((), (), s32[]{:S(2)}) async-start(), calls=%async_computation.8 | async-start | bytes 2228224 | tf_op jit(solution)/shard_map/all_gather | solution.py:86
  114.0 89.4 %copy-start.17 = (s32[256,6]{0,1:T(8,128)S(1)}, s32[256,6]{0,1:T(8,128)}, u32[]{:S(2)}) copy-start(s32[256,6]{0,1:T(8,128)} %param.11) | copy-start | bytes 18436
  194.8 87.8 %all-to-all-start.2 = ((bf16[16,128,512]{2,1,0:T(8,128)(2,1)}), bf16[16,128,512]{2,1,0:T(8,128)(2,1)}, u32[]{:S(2)}, u32[]{:S(2)}) async-start(bf16[16,128,512]{2,1,0:T(8,128)(2,1)} %convert_element_type.59), calls=%async_computation.2 | async-start | bytes 4194304 | tf_op jit(solution)/shard_map/all_to_all | solution.py:83
  202.2 266.0 %all-gather.9.cloned.1.call-start = ((), (), s32[]{:S(2)}) async-start(), calls=%async_computation.9 | async-start | bytes 2228224 | tf_op jit(solution)/shard_map/all_gather | solution.py:89
  202.2 90.2 %collective-permute-start = (bf16[2048,512]{1,0:T(8,128)(2,1)S(1)}, bf16[2048,512]{1,0:T(8,128)(2,1)}, u32[]{:S(2)}, u32[]{:S(2)}) collective-permute-start(bf16[2048,512]{1,0:T(8,128)(2,1)S(1)} %bitcast.75), channel_id=1, source_target_pairs={{0,1},{1,0},{2,3},{3,2},{4,5},{5,4},{6,7},{7,6},{8,9},{9,8},{10,11... | collective-permute-start | bytes 6291464 | tf_op jit(solution)/shard_map/ppermute | solution.py:119
  203.4 357.0 %reduce-scatter.2.cloned.1.call-start = ((), (), s32[]{:S(2)}) async-start(), calls=%async_computation.7 | async-start | bytes 8912896 | tf_op jit(solution)/shard_map/reduce_scatter | solution.py:128
  275.8 24.3 %collective-permute-start.1 = (bf16[2048,512]{1,0:T(8,128)(2,1)}, bf16[2048,512]{1,0:T(8,128)(2,1)}, u32[]{:S(2)}, u32[]{:S(2)}) collective-permute-start(bf16[2048,512]{1,0:T(8,128)(2,1)} %bitcast.1), channel_id=1, source_target_pairs={{0,1},{1,0},{2,3},{3,2},{4,5},{5,4},{6,7},{7,6},{8,9},{9,8},{10,11... | collective-permute-start | bytes 6291464 | tf_op jit(solution)/shard_map/ppermute | solution.py:120
  282.7 41.7 %collective-permute-start.2 = (bf16[2048,512]{1,0:T(8,128)(2,1)}, bf16[2048,512]{1,0:T(8,128)(2,1)}, u32[]{:S(2)}, u32[]{:S(2)}) collective-permute-start(bf16[2048,512]{1,0:T(8,128)(2,1)} %bitcast.4), channel_id=1, source_target_pairs={{0,1},{1,0},{2,3},{3,2},{4,5},{5,4},{6,7},{7,6},{8,9},{9,8},{10,11... | collective-permute-start | bytes 6291464 | tf_op jit(solution)/shard_map/ppermute | solution.py:121
  338.9 4.7 collective-permute-start.3
  343.6 17.9 %collective-permute-start.4 = (bf16[128,512]{1,0:T(8,128)(2,1)S(1)}, bf16[128,512]{1,0:T(8,128)(2,1)S(1)}, u32[]{:S(2)}, u32[]{:S(2)}) collective-permute-start(bf16[128,512]{1,0:T(8,128)(2,1)S(1)} %collective-permute-done.3), channel_id=1, source_target_pairs={{0,2},{2,4},{4,6},{6,8},{8,10},{10,12},{12,14},{14,16},{16,18},{18... | collective-permute-start | bytes 393224 | tf_op jit(solution)/shard_map/ppermute | solution.py:28
  346.2 15.3 %collective-permute-start.11 = (bf16[128,512]{1,0:T(8,128)(2,1)S(1)}, bf16[128,512]{1,0:T(8,128)(2,1)S(1)}, u32[]{:S(2)}, u32[]{:S(2)}) collective-permute-start(bf16[128,512]{1,0:T(8,128)(2,1)S(1)} %convert_element_type.68), channel_id=1, source_target_pairs={{2,0},{4,2},{6,4},{8,6},{10,8},{12,10},{14,12},{16,14},{18,16},{20... | collective-permute-start | bytes 393224 | tf_op jit(solution)/shard_map/ppermute | solution.py:32
  361.5 10.8 %collective-permute-start.5 = (bf16[128,512]{1,0:T(8,128)(2,1)S(1)}, bf16[128,512]{1,0:T(8,128)(2,1)S(1)}, u32[]{:S(2)}, u32[]{:S(2)}) collective-permute-start(bf16[128,512]{1,0:T(8,128)(2,1)S(1)} %collective-permute-done.4), channel_id=1, source_target_pairs={{0,2},{2,4},{4,6},{6,8},{8,10},{10,12},{12,14},{14,16},{16,18},{18... | collective-permute-start | bytes 393224 | tf_op jit(solution)/shard_map/ppermute | solution.py:28
  362.2 18.3 %collective-permute-start.12 = (bf16[128,512]{1,0:T(8,128)(2,1)S(1)}, bf16[128,512]{1,0:T(8,128)(2,1)S(1)}, u32[]{:S(2)}, u32[]{:S(2)}) collective-permute-start(bf16[128,512]{1,0:T(8,128)(2,1)S(1)} %collective-permute-done.11), channel_id=1, source_target_pairs={{2,0},{4,2},{6,4},{8,6},{10,8},{12,10},{14,12},{16,14},{18,16},{20... | collective-permute-start | bytes 393224 | tf_op jit(solution)/shard_map/ppermute | solution.py:32
  372.3 13.3 %collective-permute-start.6 = (bf16[128,512]{1,0:T(8,128)(2,1)S(1)}, bf16[128,512]{1,0:T(8,128)(2,1)S(1)}, u32[]{:S(2)}, u32[]{:S(2)}) collective-permute-start(bf16[128,512]{1,0:T(8,128)(2,1)S(1)} %collective-permute-done.5), channel_id=1, source_target_pairs={{0,2},{2,4},{4,6},{6,8},{8,10},{10,12},{12,14},{14,16},{16,18},{18... | collective-permute-start | bytes 393224 | tf_op jit(solution)/shard_map/ppermute | solution.py:28
  380.6 13.7 %collective-permute-start.13 = (bf16[128,512]{1,0:T(8,128)(2,1)S(1)}, bf16[128,512]{1,0:T(8,128)(2,1)S(1)}, u32[]{:S(2)}, u32[]{:S(2)}) collective-permute-start(bf16[128,512]{1,0:T(8,128)(2,1)S(1)} %collective-permute-done.12), channel_id=1, source_target_pairs={{2,0},{4,2},{6,4},{8,6},{10,8},{12,10},{14,12},{16,14},{18,16},{20... | collective-permute-start | bytes 393224 | tf_op jit(solution)/shard_map/ppermute | solution.py:32
  385.7 22.9 %copy-start.15 = (bf16[128,512]{1,0:T(8,128)(2,1)}, bf16[128,512]{1,0:T(8,128)(2,1)S(1)}, u32[]{:S(2)}) copy-start(bf16[128,512]{1,0:T(8,128)(2,1)S(1)} %collective-permute-done.6) | copy-start | bytes 393220
  385.7 15.4 %collective-permute-start.7 = (bf16[128,512]{1,0:T(8,128)(2,1)S(1)}, bf16[128,512]{1,0:T(8,128)(2,1)S(1)}, u32[]{:S(2)}, u32[]{:S(2)}) collective-permute-start(bf16[128,512]{1,0:T(8,128)(2,1)S(1)} %collective-permute-done.6), channel_id=1, source_target_pairs={{0,2},{2,4},{4,6},{6,8},{8,10},{10,12},{12,14},{14,16},{16,18},{18... | collective-permute-start | bytes 393224 | tf_op jit(solution)/shard_map/ppermute | solution.py:28
  394.2 14.4 %collective-permute-start.14 = (bf16[128,512]{1,0:T(8,128)(2,1)S(1)}, bf16[128,512]{1,0:T(8,128)(2,1)}, u32[]{:S(2)}, u32[]{:S(2)}) collective-permute-start(bf16[128,512]{1,0:T(8,128)(2,1)S(1)} %collective-permute-done.13), channel_id=1, source_target_pairs={{2,0},{4,2},{6,4},{8,6},{10,8},{12,10},{14,12},{16,14},{18,16},{20... | collective-permute-start | bytes 393224 | tf_op jit(solution)/shard_map/ppermute | solution.py:32
  401.0 15.5 %collective-permute-start.8 = (bf16[128,512]{1,0:T(8,128)(2,1)S(1)}, bf16[128,512]{1,0:T(8,128)(2,1)}, u32[]{:S(2)}, u32[]{:S(2)}) collective-permute-start(bf16[128,512]{1,0:T(8,128)(2,1)S(1)} %collective-permute-done.7), channel_id=1, source_target_pairs={{0,2},{2,4},{4,6},{6,8},{8,10},{10,12},{12,14},{14,16},{16,18},{18... | collective-permute-start | bytes 393224 | tf_op jit(solution)/shard_map/ppermute | solution.py:28
  408.6 14.2 %collective-permute-start.15 = (bf16[128,512]{1,0:T(8,128)(2,1)}, bf16[128,512]{1,0:T(8,128)(2,1)}, u32[]{:S(2)}, u32[]{:S(2)}) collective-permute-start(bf16[128,512]{1,0:T(8,128)(2,1)} %collective-permute-done.14), channel_id=1, source_target_pairs={{2,0},{4,2},{6,4},{8,6},{10,8},{12,10},{14,12},{16,14},{18,16},{20... | collective-permute-start | bytes 393224 | tf_op jit(solution)/shard_map/ppermute | solution.py:32
  416.6 12.2 %collective-permute-start.9 = (bf16[128,512]{1,0:T(8,128)(2,1)}, bf16[128,512]{1,0:T(8,128)(2,1)}, u32[]{:S(2)}, u32[]{:S(2)}) collective-permute-start(bf16[128,512]{1,0:T(8,128)(2,1)} %collective-permute-done.8), channel_id=1, source_target_pairs={{0,2},{2,4},{4,6},{6,8},{8,10},{10,12},{12,14},{14,16},{16,18},{18... | collective-permute-start | bytes 393224 | tf_op jit(solution)/shard_map/ppermute | solution.py:28
  416.6 38.4 %copy-start.8 = (bf16[128,512]{1,0:T(8,128)(2,1)S(1)}, bf16[128,512]{1,0:T(8,128)(2,1)}, u32[]{:S(2)}) copy-start(bf16[128,512]{1,0:T(8,128)(2,1)} %copy-done.7) | copy-start | bytes 393220
  416.6 39.1 %copy-start.11 = (bf16[128,512]{1,0:T(8,128)(2,1)S(1)}, bf16[128,512]{1,0:T(8,128)(2,1)}, u32[]{:S(2)}) copy-start(bf16[128,512]{1,0:T(8,128)(2,1)} %copy-done.10) | copy-start | bytes 393220
  416.6 39.8 %copy-start.14 = (bf16[128,512]{1,0:T(8,128)(2,1)S(1)}, bf16[128,512]{1,0:T(8,128)(2,1)}, u32[]{:S(2)}) copy-start(bf16[128,512]{1,0:T(8,128)(2,1)} %copy-done.13) | copy-start | bytes 393220
  422.8 15.2 %collective-permute-start.16 = (bf16[128,512]{1,0:T(8,128)(2,1)}, bf16[128,512]{1,0:T(8,128)(2,1)S(1)}, u32[]{:S(2)}, u32[]{:S(2)}) collective-permute-start(bf16[128,512]{1,0:T(8,128)(2,1)} %collective-permute-done.15), channel_id=1, source_target_pairs={{2,0},{4,2},{6,4},{8,6},{10,8},{12,10},{14,12},{16,14},{18,16},{20... | collective-permute-start | bytes 393224 | tf_op jit(solution)/shard_map/ppermute | solution.py:32
  428.8 14.8 %collective-permute-start.10 = (bf16[128,512]{1,0:T(8,128)(2,1)}, bf16[128,512]{1,0:T(8,128)(2,1)S(1)}, u32[]{:S(2)}, u32[]{:S(2)}) collective-permute-start(bf16[128,512]{1,0:T(8,128)(2,1)} %collective-permute-done.9), channel_id=1, source_target_pairs={{0,2},{2,4},{4,6},{6,8},{8,10},{10,12},{12,14},{14,16},{16,18},{18... | collective-permute-start | bytes 393224 | tf_op jit(solution)/shard_map/ppermute | solution.py:28
  438.0 22.8 %collective-permute-start.17 = (bf16[128,512]{1,0:T(8,128)(2,1)S(1)}, bf16[128,512]{1,0:T(8,128)(2,1)S(1)}, u32[]{:S(2)}, u32[]{:S(2)}) collective-permute-start(bf16[128,512]{1,0:T(8,128)(2,1)S(1)} %collective-permute-done.16), channel_id=1, source_target_pairs={{2,0},{4,2},{6,4},{8,6},{10,8},{12,10},{14,12},{16,14},{18,16},{20... | collective-permute-start | bytes 393224 | tf_op jit(solution)/shard_map/ppermute | solution.py:32
  475.2 6.4 %all-to-all-start.4 = ((bf16[2,256,1024]{2,1,0:T(8,128)(2,1)}), bf16[2,256,1024]{2,1,0:T(8,128)(2,1)S(1)}, u32[]{:S(2)}, u32[]{:S(2)}) async-start(bf16[2,256,1024]{2,1,0:T(8,128)(2,1)} %bitcast.78), calls=%async_computation.5 | async-start | bytes 2097152 | tf_op jit(solution)/shard_map/all_to_all | solution.py:100
  482.7 83.5 %copy-start.2 = (f32[256,1024]{1,0:T(8,128)S(1)}, f32[256,1024]{1,0:T(8,128)}, u32[]{:S(2)}) copy-start(f32[256,1024]{1,0:T(8,128)} %convert_reduce_fusion) | copy-start | bytes 3145732
  (13 other events, 77.9 us)
Sparse Core Ops, SparseCore 0:
  11.3 181.4 all-gather.4
  195.6 81.2 all-gather.6
  279.7 59.4 all-gather.8
  341.3 218.9 reduce-scatter.1
